TPU v7x, 32 devices: a whole 2x2x4 slice. The times are simulated.
32 devices in a mesh: grp: 2 (over y), fs: 4 (over z), tp: 4 (over x, core).
Axes of the slice: x: 2, y: 2, z: 4, core: 2. Of those that a mesh axis runs over, the one named last changes fastest.
Arguments:
- tokens: bfloat16 [1792, 2048], P(('grp', 'fs'), 'tp'), parts along dimension 0, may hold values from -6 to 6
- route_ids: int32 [1792, 2], P(('grp', 'fs')), parts along dimension 0, may hold values from 0 to 3, all different within a row; in each aligned block of 224 rows (0 to 223, 224 to 447, ...) at most 168 rows name the same one
- route_weights: float32 [1792, 2], P(('grp', 'fs')), parts along dimension 0, may hold values from 0.25 to 1
- norm_gain: float32 [2048], P('fs'), may hold values from 0.1 to 1.9
- gate_master: float32 [4, 2048, 512], P(None, 'fs', 'tp'), may hold values from -0.125 to 0.125
- up_master: float32 [4, 2048, 512], P(None, 'fs', 'tp'), may hold values from -0.125 to 0.125
- down_master: float32 [4, 2048, 512], P(None, 'fs', 'tp'), may hold values from -0.25 to 0.25
Outputs:
- gate_serve: bfloat16 [8, 2048, 512], P(('grp', 'fs'), None, 'tp'), parts along dimension 0
- up_serve: bfloat16 [8, 2048, 512], P(('grp', 'fs'), None, 'tp'), parts along dimension 0
- down_serve: bfloat16 [8, 2048, 512], P(('grp', 'fs'), None, 'tp'), parts along dimension 0
- moe_output: bfloat16 [1792, 2048], P(('grp', 'fs'), 'tp'), parts along dimension 0
There are 2 independent parts, one for each index of `grp`. A program takes and returns all parts, laid end to end along the dimension named above; an argument that names none is the same for every part. Nothing has to cross between parts.
Inputs may be any that keep to these rules, and one draw needn't show every extreme that they name: `route_ids`: the 2 experts of a row differ; within the rows of one index of fs (aligned blocks of 224 rows) no expert is named more than 168 times.
All inputs are finite; a program needn't handle non-finite values.
Results may differ from a plain program's by a relative error of at most 0.012.
Values may be sent and summed in bfloat16 or wider, within the bound.
A program may use at most 64 MiB of HBM per device.

v0:
```python
import jax
import jax.numpy as jnp
from jax import lax
from jax.experimental import pallas as pl
from jax.experimental.pallas import tpu as pltpu
from jax.sharding import PartitionSpec as P

norm_epsilon = 1e-06


def slot_numbers(route_ids, experts, capacity):
    flat_ids = route_ids.reshape(-1)
    onehot = (flat_ids[:, None] == jnp.arange(experts, dtype=jnp.int32)[None, :]).astype(jnp.int32)
    before = jnp.cumsum(onehot, axis=0) - onehot
    position = jnp.sum(before * onehot, axis=1)
    return (flat_ids * capacity + position).reshape(route_ids.shape)


def local(tokens, route_ids, route_weights, norm_gain, gate_master, up_master, down_master):
    experts = gate_master.shape[0]
    shards = lax.axis_size("fs")
    columns = lax.axis_size("tp")
    per_device = experts // shards
    tok_rows = route_ids.shape[0]
    top_count = route_ids.shape[1]
    local_width = tokens.shape[1]
    model_width = local_width * columns
    capacity = max(2, 3 * tok_rows * top_count // (2 * experts))
    row_gain = norm_gain[None, :, None]
    gate_half = (gate_master * row_gain).astype(jnp.bfloat16)
    up_half = (up_master * row_gain).astype(jnp.bfloat16)
    down_half = down_master.astype(jnp.bfloat16)
    gate_serve, up_serve, down_serve = (
        lax.all_to_all(gate_half, "fs", split_axis=0, concat_axis=1, tiled=True),
        lax.all_to_all(up_half, "fs", split_axis=0, concat_axis=1, tiled=True),
        lax.all_to_all(down_half, "fs", split_axis=0, concat_axis=1, tiled=True),
    )
    slot_ids = slot_numbers(route_ids, experts, capacity)
    slot_range = jnp.arange(experts * capacity, dtype=jnp.int32)
    selects = [
        (slot_ids[:, rank_slot, None] == slot_range[None, :]).astype(jnp.bfloat16)
        for rank_slot in range(top_count)
    ]
    placing = selects[0]
    for extra in selects[1:]:
        placing = placing + extra
    local_values = tokens.astype(jnp.float32)
    squares = lax.psum(jnp.sum(local_values * local_values, axis=1), "tp")
    inverse = lax.rsqrt(squares / model_width + norm_epsilon)[:, None]
    normed = (local_values * inverse).astype(jnp.bfloat16)
    buffer = jnp.einsum("ts,td->sd", placing, normed, preferred_element_type=jnp.float32).astype(
        jnp.bfloat16
    )
    arrived = lax.all_to_all(
        buffer.reshape(shards, per_device * capacity, local_width),
        "fs",
        split_axis=0,
        concat_axis=0,
        tiled=True,
    )
    arrived = arrived.reshape(shards, per_device, capacity, local_width)
    partial_value = lax.all_gather(arrived, "tp", axis=3, tiled=True)
    gate_sum = jnp.einsum(
        "sxcd,xdf->xscf", partial_value, gate_serve, preferred_element_type=jnp.float32
    )
    up_sum = jnp.einsum(
        "sxcd,xdf->xscf", partial_value, up_serve, preferred_element_type=jnp.float32
    )
    hidden = (jax.nn.silu(gate_sum) * up_sum).astype(jnp.bfloat16)
    products = jnp.einsum("xdf,xscf->dsxc", down_serve, hidden, preferred_element_type=jnp.float32)
    summed = lax.psum_scatter(
        products.reshape(local_width * lax.axis_size("tp"), shards * per_device * capacity).astype(
            jnp.bfloat16
        ),
        "tp",
        scatter_dimension=0,
        tiled=True,
    )
    returned = lax.all_to_all(
        summed.reshape(local_width, shards, per_device * capacity),
        "fs",
        split_axis=1,
        concat_axis=1,
        tiled=True,
    )
    returned = returned.reshape(local_width, experts * capacity)
    combined = jnp.zeros((tok_rows, local_width), jnp.float32)
    for rank_slot in range(top_count):
        picked = jnp.einsum(
            "ts,ds->td", selects[rank_slot], returned, preferred_element_type=jnp.float32
        )
        combined = combined + route_weights[:, rank_slot : rank_slot + 1] * picked
    return (gate_serve, up_serve, down_serve, combined.astype(jnp.bfloat16))


MESH = pl.DeviceIdType.MESH
bf16, f32, i32 = jnp.bfloat16, jnp.float32, jnp.int32
GU_CUT, TOK_CUT = 2, 2
MATE_CUTS, FAR_CUTS = (2, 2), (4, 4, 4, 8, 8)


def remote(src, dst, send, recv, to):
    return pltpu.make_async_remote_copy(
        src_ref=src, dst_ref=dst, send_sem=send, recv_sem=recv, device_id=to, device_id_type=MESH
    )


def kernel(
    tokens, ids_h, weights_h, gain_h, gm, um, dm,
    wgu, wd, moe,
    xt, ids, weights, gain, gcol, mv, sgu, sd, acc, inv, scale, wrow, wsend, hid,
    ss, sr, xs, xr, keep, zs, zr,
    in_sem, ld_sem, sent, c_recv, w_recv, p_recv, gu_recv, guy_recv,
    mate_recv, mate_y, far_recv, far_y, s_recv, x_recv, z_recv,
):
    g, f, t = lax.axis_index("grp"), lax.axis_index("fs"), lax.axis_index("tp")
    H, Fl = mv.shape[2:]
    Dl = 2 * H
    T, Dq = tokens.shape
    NT = xt.shape[0]
    D = NT * Dq
    Rg = H // GU_CUT
    to_gu, to_dn, to_guy, to_dny, to_tok, to_w, to_tp, to_swap, to_x, to_z = (
        sent.at[i] for i in range(10)
    )
    units = Dl // Fl
    per_half = units // 2
    pair, me = f // 2, lax.rem(f, 2)
    chip, core = t // 2, lax.rem(t, 2)
    mate = f + 1 - 2 * me
    twin = f + 2 - 4 * pair
    mate_twin = mate + 2 - 4 * pair
    far_a, far_b = 2 - pair, 3 - 3 * pair
    sib, over = {"tp": t + 1 - 2 * core}, {"tp": t + 2 - 4 * chip}
    peer, to_mate = {"grp": 1 - g}, {"fs": mate}
    mine_rows, mate_rows = (pl.ds(pl.multiple_of(i * T, T), T) for i in (me, 1 - me))

    inner = (f + 1) // 2 % 2 == 1
    home = chip == pair
    own_mine = core == me

    def cut(s, half, p, n):
        return pl.ds(pl.multiple_of(s * Dl + half * H + p * n, n), n)

    def spans(cuts):
        at, out = 0, []
        for c in cuts:
            out.append((at, H // c))
            at += H // c
        return out

    mate_spans, far_spans = spans(MATE_CUTS), spans(FAR_CUTS)

    def span(s, half, at, n):
        return pl.ds(pl.multiple_of(s * Dl + half * H + at, n), n)

    is_inner = (f + 1) // 2 % 2
    kind_a, kind_b = is_inner, 1 - is_inner

    def both(s):
        return pl.ds(pl.multiple_of(s * Dl, Dl), Dl)

    small = [
        pltpu.make_async_copy(gain_h, gain, in_sem.at[0]),
        pltpu.make_async_copy(tokens, xt.at[t, mine_rows, :], in_sem.at[1]),
        pltpu.make_async_copy(ids_h, ids, in_sem.at[2]),
        pltpu.make_async_copy(weights_h, weights, in_sem.at[3]),
    ]
    for cp in small:
        cp.start()
    picks = [
        (1 - me, g), (1 - me + 2, g), (me, g), (me + 2, g), (me, 1 - g), (me + 2, 1 - g),
    ]
    loads = {}
    for k, m in [(k, m) for k in (0, 2, 1, 3) for m in (0, 1)] + [
        (k, 2) for k in (0, 1, 2, 3)
    ] + [(k, m) for k in (4, 5) for m in (0, 1, 2)]:
        e, half = picks[k]
        loads[k, m] = pltpu.make_async_copy(
            (gm, um, dm)[m].at[e, pl.ds(pl.multiple_of(half * H, H), H), :],
            mv.at[m, k], ld_sem.at[5 if k > 3 else 4 if m == 2 else k],
        )
        loads[k, m].start()

    barrier = pltpu.get_barrier_semaphore()
    friends = [to_mate, {"fs": twin}, {"fs": mate_twin}, peer, sib, over]
    for who in friends:
        pl.semaphore_signal(barrier, inc=1, device_id=who, device_id_type=MESH)

    small[0].wait()
    gcol[...] = jnp.transpose(jnp.broadcast_to(gain[...], (Fl, Dl)))
    mine_half = pl.ds(pl.multiple_of(g * H, H), H)
    other_half = pl.ds(pl.multiple_of((1 - g) * H, H), H)
    small[2].wait()
    small[3].wait()
    wrow[me] = jnp.zeros(wsend.shape, f32)
    wsend[...] = jnp.zeros(wsend.shape, f32)
    for slot in range(2):
        for ref, parity in ((wrow.at[me], me), (wsend, 1 - me)):
            row = jnp.where(ids[...] == parity + 2 * slot, weights[...], 0.0)
            ref[slot : slot + 1, :T] = jnp.sum(row, axis=0, keepdims=True)
    small[1].wait()
    pl.semaphore_wait(barrier, len(friends))
    w_hop = remote(wsend, wrow.at[me], to_w, w_recv, to_mate)
    w_hop.start()


    Tp = T // TOK_CUT

    def tok(q, i, p):
        return xt.at[q, pl.ds(pl.multiple_of(i * T + p * Tp, Tp), Tp), :]

    def token_hop(i, p):
        return remote(tok(t, i, p), tok(t, i, p), to_tok, c_recv.at[p], to_mate)

    def spread(i, p):
        block = tok(t, i, p)
        remote(block, block, to_tp, p_recv.at[0, i, p], over).start()
        remote(block, block, to_tp, p_recv.at[1, i, p], sib).start()

    def landed(way, q, i, p):
        block = tok(q, i, p)
        remote(block, block, to_tp, p_recv.at[way, i, p], sib).wait_recv()

    def pass_on(i):
        q = t + 2 - 4 * chip
        for p in range(TOK_CUT):
            landed(0, q, i, p)
            block = tok(q, i, p)
            remote(block, block, to_tp, p_recv.at[2, i, p], sib).start()

    def sib_arrived(i):
        for p in range(TOK_CUT):
            landed(1, t + 1 - 2 * core, i, p)
            landed(2, t + 2 - 4 * chip + 1 - 2 * core, i, p)

    def gu_copy(kind, slot, p):
        src = (
            wgu.at[slot, cut(f, g, p, Rg), :] if kind == 0 else sgu.at[slot, p * Rg : (p + 1) * Rg, :]
        )
        return remote(
            src, wgu.at[slot, cut(f, g, p, Rg), :], to_gu, gu_recv.at[kind, slot, p],
            {"fs": (twin, mate_twin, mate)[kind]},
        )

    def dn_copy(kind, p):
        at, n = (mate_spans if kind == 2 else far_spans)[p]
        there = wd.at[span(f, g, at, n), :]
        src = there if kind == 0 else sd.at[at : at + n, :]
        recv = mate_recv.at[p] if kind == 2 else far_recv.at[kind, p]
        return remote(src, there, to_dn, recv, {"fs": (twin, mate_twin, mate)[kind]})

    def send_gu(slot, kinds):
        for p in range(GU_CUT):
            for kind in kinds:
                gu_copy(kind, slot, p).start()

    def send_far():
        for p in range(len(far_spans)):
            for kind in (0, 1):
                dn_copy(kind, p).start()

    def send_mate():
        for p in range(len(mate_spans)):
            dn_copy(2, p).start()

    def loaded(block, i):
        pltpu.make_async_copy(block, block, ld_sem.at[i]).wait()

    def gu_ready(slot, k, dst, part):
        if k < 4:
            loaded(mv.at[:2, k], k)
        dst[:, :Fl] = (mv[0, k] * gcol[part, :]).astype(bf16)
        dst[:, Fl:] = (mv[1, k] * gcol[part, :]).astype(bf16)

    own_gu = [wgu.at[slot, cut(f, g, 0, H), :] for slot in range(2)]
    gu_ready(0, 0, sgu.at[0], mine_half)
    send_gu(0, (2,))
    for p in range(TOK_CUT):
        token_hop(me, p).start()
        spread(me, p)

    @pl.when(inner)
    def _():
        send_gu(0, (1,))

    gu_ready(0, 2, own_gu[0], mine_half)

    @pl.when(inner)
    def _():
        send_gu(0, (0,))

    gu_ready(1, 1, sgu.at[1], mine_half)
    send_gu(1, (2,))

    @pl.when(inner)
    def _():
        send_gu(1, (1,))

    gu_ready(1, 3, own_gu[1], mine_half)

    @pl.when(inner)
    def _():
        send_gu(1, (0,))

    @pl.when(jnp.logical_not(inner))
    def _():
        send_gu(0, (0, 1))
        send_gu(1, (0, 1))

    loaded(mv.at[2, :4], 4)
    for slot in range(2):
        lanes = slice(slot * Fl, (slot + 1) * Fl)
        sd[:, lanes] = mv[2, slot].astype(bf16)
        wd[cut(f, g, 0, H), lanes] = mv[2, 2 + slot].astype(bf16)
    send_mate()

    @pl.when(jnp.logical_not(inner))
    def _():
        send_far()

    loaded(mv.at[:, 4:], 5)
    for slot in range(2):
        lanes = slice(slot * Fl, (slot + 1) * Fl)
        gu_ready(slot, 4 + slot, wgu.at[slot, cut(f, 1 - g, 0, H), :], other_half)
        wd[cut(f, 1 - g, 0, H), lanes] = mv[2, 4 + slot].astype(bf16)

    def gu_forward(kind, slot, p):
        here = wgu.at[slot, cut(origin(kind), g, p, Rg), :]
        landing, onward = gu_recv.at[kind, slot, p], guy_recv.at[kind, slot, p]
        remote(here, here, to_guy, landing, peer).wait_recv()
        remote(here, here, to_guy, onward, peer).start()

    def gu_peer(kind, slot):
        for p in range(GU_CUT):
            there = wgu.at[slot, cut(origin(kind), 1 - g, p, Rg), :]
            remote(there, there, to_guy, guy_recv.at[kind, slot, p], peer).wait_recv()

    def origin(kind):
        return mate if isinstance(kind, int) else far_a if kind is kind_a else far_b

    def mate_forward():
        for p, (at, n) in enumerate(mate_spans):
            here = wd.at[span(mate, g, at, n), :]
            remote(here, here, to_dny, mate_recv.at[p], peer).wait_recv()
            remote(here, here, to_dny, mate_y.at[p], peer).start()

    def mate_peer():
        for p, (at, n) in enumerate(mate_spans):
            there = wd.at[span(mate, 1 - g, at, n), :]
            remote(there, there, to_dny, mate_y.at[p], peer).wait_recv()

    def far_forward(*pieces):
        for p in pieces:
            for kind, s in ((kind_a, far_a), (kind_b, far_b)):
                here = wd.at[span(s, g, *far_spans[p]), :]
                remote(here, here, to_dny, far_recv.at[kind, p], peer).wait_recv()
                remote(here, here, to_dny, far_y.at[kind, p], peer).start()

    def far_peer(*pieces):
        for p in pieces:
            for kind, s in ((kind_a, far_a), (kind_b, far_b)):
                there = wd.at[span(s, 1 - g, *far_spans[p]), :]
                remote(there, there, to_dny, far_y.at[kind, p], peer).wait_recv()

    def gu_all(kind, slot):
        for p in range(GU_CUT):
            gu_forward(kind, slot, p)

    def partial_sums(s, slot):
        return jnp.dot(xt[s], wgu[slot, both(s), :], preferred_element_type=f32)

    gu_all(2, 0)
    gu_all(kind_a, 0)
    gu_all(kind_a, 1)
    pass_on(me)
    for p in range(TOK_CUT):
        token_hop(1 - me, p).wait_recv()
        spread(1 - me, p)

    @pl.when(inner)
    def _():
        gu_all(2, 1)
        gu_all(kind_b, 0)
        pass_on(1 - me)
        gu_forward(kind_b, 1, 0)
        send_far()
        for p in range(1, GU_CUT):
            gu_forward(kind_b, 1, p)

    @pl.when(jnp.logical_not(inner))
    def _():
        gu_all(kind_b, 0)
        for p in range(GU_CUT):
            gu_forward(2, 1, p)
            if p == 0:
                pass_on(1 - me)
            gu_forward(kind_b, 1, p)

    remote(wsend, wrow.at[1 - me], w_recv, w_recv, to_mate).wait_recv()
    sib_arrived(me)
    sib_arrived(1 - me)
    for i in range(2):
        rows = slice(i * T, (i + 1) * T)
        sq = jnp.zeros((T, Fl), f32)
        for q in range(NT):
            for c in range(Dq // Fl):
                part = xt[q, rows, c * Fl : (c + 1) * Fl].astype(f32)
                sq = sq + part * part
        root = lax.rsqrt(jnp.sum(sq, axis=1, keepdims=True) / D + norm_epsilon)
        inv[rows, :] = jnp.broadcast_to(root, (T, Fl))
        for slot in range(2):
            wide = jnp.transpose(
                jnp.broadcast_to(wrow[i, slot : slot + 1, :], (Fl, wrow.shape[2]))
            )
            scale[slot, rows, :] = wide[:T] * root

    for slot in range(2):
        acc[slot] = partial_sums(f, slot)
    for kind, s in ((kind_a, far_a), (2, mate)):
        for slot in range(2):
            gu_peer(kind, slot)
            acc[slot] += partial_sums(s, slot)

    def hidden(slot):
        gu_peer(kind_b, slot)
        sums = acc[slot] + partial_sums(far_b, slot)
        gate, up = sums[:, :Fl] * inv[...], sums[:, Fl:] * scale[slot]
        hid[:, slot * Fl : (slot + 1) * Fl] = (gate / (1.0 + jnp.exp(-gate)) * up).astype(bf16)

    near_mine, near_theirs = 2 * pair + core, 2 * pair + 1 - core
    far_mine, far_theirs = 2 - 2 * pair + core, 2 - 2 * pair + 1 - core

    def out_part(s, u, n):
        rows = pl.ds(pl.multiple_of(s * Dl + u * Fl, Fl), n * Fl)
        return lax.dot_general(
            hid[...], wd[rows, :], (((1,), (1,)), ((), ())), preferred_element_type=f32
        )

    def swap(n, u, count, i):
        at = pl.ds(u, count)
        return remote(ss.at[n, at], sr.at[n, at], to_swap, s_recv.at[i], sib)

    def cross(n, u, count, rows, i):
        at = pl.ds(u, count)
        return remote(xs.at[n, at, :rows], xr.at[n, at, :rows], to_x, x_recv.at[i], over)

    def back(n, u, count, i):
        at = pl.ds(u, count)
        return remote(zs.at[n, at], zr.at[n, at], to_z, z_recv.at[i], to_mate)

    class Unit:
        def __init__(self, n, u, count, i, x_first):
            self.n, self.u, self.count, self.i, self.x_first = n, u, count, i, x_first
            self.theirs, self.mine = ((near_theirs, near_mine), (far_theirs, far_mine))[n]
            self.kept = home if n == 0 else jnp.logical_not(home)
            self.at = [u + c for c in range(count)]
            self.cross = cross(n, u, count, 2 * T if x_first else T, i)
            self.back = back(n, u, count, i)
            self.swap = swap(n, u, count, i)

        def give(self):
            y = out_part(self.theirs, self.u, self.count)
            for c, at in enumerate(self.at):
                ss[self.n, at] = y[:, c * Fl : (c + 1) * Fl].astype(bf16)
            self.swap.start()

        def sum(self):
            y = out_part(self.mine, self.u, self.count)
            self.swap.wait_recv()
            for c, at in enumerate(self.at):
                keep[self.n, at] = y[:, c * Fl : (c + 1) * Fl] + sr[self.n, at].astype(f32)

        def send(self):
            if self.x_first:
                @pl.when(jnp.logical_not(self.kept))
                def _():
                    for at in self.at:
                        xs[self.n, at] = keep[self.n, at].astype(bf16)
                    self.cross.start()
            else:
                for at in self.at:
                    zs[self.n, at] = keep[self.n, at, mate_rows, :].astype(bf16)
                self.back.start()

        def second(self):
            n = self.n
            if self.x_first:
                @pl.when(self.kept)
                def _():
                    self.cross.wait_recv()
                    for at in self.at:
                        zs[n, at] = (
                            keep[n, at, mate_rows, :] + xr[n, at, mate_rows, :].astype(f32)
                        ).astype(bf16)
                    self.back.start()
            else:
                @pl.when(jnp.logical_not(self.kept))
                def _():
                    self.back.wait_recv()
                    for at in self.at:
                        xs[n, at, :T] = (keep[n, at, mine_rows, :] + zr[n, at].astype(f32)).astype(bf16)
                    self.cross.start()

        def last(self):
            n = self.n

            @pl.when(self.kept)
            def _():
                self.back.wait_recv()
                if not self.x_first:
                    self.cross.wait_recv()
                for at in self.at:
                    other = xr[n, at, mine_rows, :] if self.x_first else xr[n, at, :T]
                    lanes = pl.ds(pl.multiple_of(at * Fl, Fl), Fl)
                    moe[:, lanes] = (
                        keep[n, at, mine_rows, :] + other.astype(f32) + zr[n, at].astype(f32)
                    ).astype(bf16)

    near = [Unit(0, half * per_half, per_half, half, half == 0) for half in range(2)]
    far = [
        Unit(1, half * per_half + j, 1, 2 + k * per_half + j, j % 2 == 0)
        for k, half in enumerate((g, 1 - g)) for j in range(per_half)
    ]
    pieces = range(len(far_spans))
    first_pieces = [p for p in pieces if far_spans[p][0] < H // 2]
    last_pieces = [p for p in pieces if p not in first_pieces]

    mate_forward()
    hidden(0)
    hidden(1)

    def near_give(mine_first):
        @pl.when(own_mine if mine_first else jnp.logical_not(own_mine))
        def _():
            for unit in near:
                unit.give()

    def near_sum(mine_first):
        @pl.when(own_mine if mine_first else jnp.logical_not(own_mine))
        def _():
            for unit in near:
                unit.sum()
            near[0].send()

    near_give(False)

    @pl.when(inner)
    def _():
        near_sum(True)
        mate_peer()
        near_give(True)
        far_forward(*first_pieces[:1])
        near_sum(False)
        far_forward(*first_pieces[1:])

    @pl.when(jnp.logical_not(inner))
    def _():
        far_forward(*first_pieces[:1])
        near_sum(True)
        far_forward(*first_pieces[1:])
        mate_peer()
        near_give(True)
        near_sum(False)

    far[0].give()
    far_forward(*last_pieces)
    near[1].send()
    far[1].give()
    far[0].sum()
    far[0].send()
    far_peer(*first_pieces)
    far[2].give()
    far[1].sum()
    far[1].send()
    far[2].sum()
    far[2].send()
    far_peer(*last_pieces)
    far[3].give()
    far[3].sum()
    far[3].send()
    for unit in near + far:
        unit.second()
    for unit in far + near:
        unit.last()

    def all_sent(block, sem):
        pltpu.make_async_copy(block, block, sem).wait()

    w_hop.wait_send()
    for block, sem in (
        (wgu.at[:, : 3 * H, :], to_gu), (wgu.at[:, : 3 * H, :], to_guy),
        (wd.at[: 3 * H, :], to_dn), (wd.at[: 3 * H, :], to_dny),
        (xt.at[0, :T, :], to_tok), (xt.at[:3], to_tp), (ss, to_swap),
        (xs.at[0, : 3 * units // 4], to_x), (zs.at[:, : 3 * units // 4], to_z),
    ):
        all_sent(block, sem)


def finish_kernel(wgu, wd, moe, gate_o, up_o, down_o, moe_o, sems):
    Fl = gate_o.shape[2]
    slot = lax.axis_index("fs") // 2
    lanes = pl.ds(pl.multiple_of(slot * Fl, Fl), Fl)
    copies = [
        pltpu.make_async_copy(wgu.at[slot, :, :Fl], gate_o.at[0], sems.at[0]),
        pltpu.make_async_copy(wgu.at[slot, :, Fl:], up_o.at[0], sems.at[1]),
        pltpu.make_async_copy(wd.at[:, lanes], down_o.at[0], sems.at[2]),
        pltpu.make_async_copy(moe, moe_o, sems.at[3]),
    ]
    for cp in copies:
        cp.start()
    for cp in copies:
        cp.wait()


def fused(tokens, route_ids, route_weights, norm_gain, gate_master, up_master, down_master):
    NF, NT = lax.axis_size("fs"), lax.axis_size("tp")
    E, Dl, Fl = gate_master.shape
    T, Dq = tokens.shape
    K = route_ids.shape[1]
    H = Dl // 2
    D = Dl * NF
    Tw = -(-T // 128) * 128
    units = Dl // Fl
    dma = pltpu.SemaphoreType.DMA
    vmem, hbm = pl.BlockSpec(memory_space=pltpu.VMEM), pl.BlockSpec(memory_space=pl.ANY)
    gu = (3, 2, GU_CUT)
    ins = (
        tokens, route_ids.T, route_weights.T, norm_gain[None, :],
        gate_master, up_master, down_master,
    )
    done = pl.pallas_call(
        kernel,
        out_shape=(
            pltpu.VMEM((2, D, 2 * Fl), bf16), pltpu.VMEM((D, 2 * Fl), bf16), pltpu.VMEM((T, Dq), bf16),
        ),
        in_specs=[hbm] * 7,
        out_specs=(vmem,) * 3,
        scratch_shapes=[
            pltpu.VMEM((NT, 2 * T, Dq), bf16),
            pltpu.VMEM((K, T), i32),
            pltpu.VMEM((K, T), f32),
            pltpu.VMEM((1, Dl), f32),
            pltpu.VMEM((Dl, Fl), f32),
            pltpu.VMEM((3, 6, H, Fl), f32),
            pltpu.VMEM((2, H, 2 * Fl), bf16),
            pltpu.VMEM((H, 2 * Fl), bf16),
            pltpu.VMEM((2, 2 * T, 2 * Fl), f32),
            pltpu.VMEM((2 * T, Fl), f32),
            pltpu.VMEM((2, 2 * T, Fl), f32),
            pltpu.VMEM((2, 8, Tw), f32),
            pltpu.VMEM((8, Tw), f32),
            pltpu.VMEM((2 * T, 2 * Fl), bf16),
            pltpu.VMEM((2, units, 2 * T, Fl), bf16),
            pltpu.VMEM((2, units, 2 * T, Fl), bf16),
            pltpu.VMEM((2, units, 2 * T, Fl), bf16),
            pltpu.VMEM((2, units, 2 * T, Fl), bf16),
            pltpu.VMEM((2, units, 2 * T, Fl), f32),
            pltpu.VMEM((2, units, T, Fl), bf16),
            pltpu.VMEM((2, units, T, Fl), bf16),
            dma((4,)), dma((6,)), dma((10,)),
            dma((TOK_CUT,)), dma(()), dma((3, 2, TOK_CUT)),
            dma(gu), dma(gu),
            dma((len(MATE_CUTS),)), dma((len(MATE_CUTS),)),
            dma((2, len(FAR_CUTS))), dma((2, len(FAR_CUTS))),
            dma((2 + units,)), dma((2 + units,)), dma((2 + units,)),
        ],
        compiler_params=pltpu.CompilerParams(
            collective_id=0, has_side_effects=True, vmem_limit_bytes=48 * 1024 * 1024
        ),
    )(*[pltpu.with_memory_space_constraint(a, pltpu.HBM) for a in ins])
    serve = jax.ShapeDtypeStruct((1, D, Fl), bf16)
    return pl.pallas_call(
        finish_kernel,
        out_shape=(serve, serve, serve, jax.ShapeDtypeStruct((T, Dq), bf16)),
        in_specs=[vmem] * 3,
        out_specs=(hbm,) * 4,
        scratch_shapes=[dma((4,))],
    )(*[pltpu.with_memory_space_constraint(a, pltpu.VMEM) for a in done])


def solution(mesh):
    shape = mesh.shape
    fits = shape['grp'] == 2 and shape['tp'] == shape['fs'] == 4
    body = fused if fits else local
    placed = (
        P(("grp", "fs"), "tp"),
        P(("grp", "fs"), None),
        P(("grp", "fs"), None),
        P("fs"),
        P(None, "fs", "tp"),
        P(None, "fs", "tp"),
        P(None, "fs", "tp"),
    )
    return jax.shard_map(
        body,
        mesh=mesh,
        in_specs=placed,
        out_specs=(
            P(("grp", "fs"), None, "tp"),
            P(("grp", "fs"), None, "tp"),
            P(("grp", "fs"), None, "tp"),
            P(("grp", "fs"), "tp"),
        ),
        check_vma=False,
    )
```

profile of v0, /device:TPU:0, one launch (start us, length us, event | category | flops | bytes accessed | tf_op | source)
XLA Modules:
  0.0 53.8 jit_solution(8161900031173279921)
XLA Ops:
  0.6 51.9 %shard_map.102 = (bf16[2,2048,256]{2,1,0:T(8,128)(2,1)S(1)}, bf16[2048,256]{1,0:T(8,128)(2,1)S(1)}, bf16[224,512]{1,0:T(8,128)(2,1)S(1)}) custom-call(bf16[224,512]{1,0:T(8,128)(2,1)} %tokens.1, s32[2,224]{1,0:T(2,128)} %bitcast.3, f32[2,224]{1,0:T(2,128)} %bitcast.4, f32[1,512]{1,0:T(1,128)} %bitcast.5, f32[4,512,128]{2,1,0:T(8,128)} %gm.1, ...), custom_call_target="tpu_custom_call" | custom-call | tf_op jit(solution)/shard_map/pallas_call | solution.py:632
  52.6 1.3 %shard_map.103 = (bf16[1,2048,128]{2,1,0:T(8,128)(2,1)}, bf16[1,2048,128]{2,1,0:T(8,128)(2,1)}, bf16[1,2048,128]{2,1,0:T(8,128)(2,1)}, bf16[224,512]{1,0:T(8,128)(2,1)}) custom-call(bf16[2,2048,256]{2,1,0:T(8,128)(2,1)S(1)} %get-tuple-element.7.wgu, bf16[2048,256]{1,0:T(8,128)(2,1)S(1)} %get-tuple-element.8.wd, bf16[224,512]{1,0:T(8,128)(2,1)S(1)} %get-tuple-element.9.moe), custom_call_target="tpu_custom_call" | custom-call | tf_op jit(solution)/shard_map/pallas_call | solution.py:673
where the time goes:
time: 54 us; the launch traced here: 53.8 us
  Pallas kernels  53.2 us (99%)
  between operations  0.64 us (1%)
    pallas_call x1, Pallas kernels, fused(): pl.pallas_call(kernel, out_shape=(pltpu.VMEM((2, D, 2 * Fl), bf16), pltpu...  51.9 us
    pallas_call x1, Pallas kernels, fused(): pl.pallas_call(finish_kernel, out_shape=(serve, serve, serve, jax.ShapeDt...  1.26 us

commit v1 on v0

--- a/solution.py
+++ b/solution.py
@@ -96,7 +96,8 @@
 MESH = pl.DeviceIdType.MESH
 bf16, f32, i32 = jnp.bfloat16, jnp.float32, jnp.int32
 GU_CUT, TOK_CUT = 2, 2
-MATE_CUTS, FAR_CUTS = (2, 2), (4, 4, 4, 8, 8)
+FAR_CUTS = (4, 4, 4, 8, 8)
+NEAR_X, FAR_X = (True, False), (True, False, True, False)
 
 
 def remote(src, dst, send, recv, to):
@@ -108,10 +109,10 @@
 def kernel(
     tokens, ids_h, weights_h, gain_h, gm, um, dm,
     wgu, wd, moe,
-    xt, ids, weights, gain, gcol, mv, sgu, sd, acc, inv, scale, wrow, wsend, hid,
+    xt, ids, weights, gain, gcol, mv, mvd, sgu, sd, acc, inv, scale, wrow, wsend, hid,
     ss, sr, xs, xr, keep, zs, zr,
     in_sem, ld_sem, sent, c_recv, w_recv, p_recv, gu_recv, guy_recv,
-    mate_recv, mate_y, far_recv, far_y, s_recv, x_recv, z_recv,
+    mate_recv, far_recv, far_y, s_recv, x_recv, z_recv,
 ):
     g, f, t = lax.axis_index("grp"), lax.axis_index("fs"), lax.axis_index("tp")
     H, Fl = mv.shape[2:]
@@ -149,7 +150,7 @@
             at += H // c
         return out
 
-    mate_spans, far_spans = spans(MATE_CUTS), spans(FAR_CUTS)
+    far_spans = spans(FAR_CUTS)
 
     def span(s, half, at, n):
         return pl.ds(pl.multiple_of(s * Dl + half * H + at, n), n)
@@ -170,15 +171,17 @@
         cp.start()
     picks = [
         (1 - me, g), (1 - me + 2, g), (me, g), (me + 2, g), (me, 1 - g), (me + 2, 1 - g),
+        (1 - me, 1 - g), (1 - me + 2, 1 - g),
     ]
     loads = {}
     for k, m in [(k, m) for k in (0, 2, 1, 3) for m in (0, 1)] + [
-        (k, 2) for k in (0, 1, 2, 3)
+        (k, 2) for k in (0, 1, 2, 3, 6, 7)
     ] + [(k, m) for k in (4, 5) for m in (0, 1, 2)]:
         e, half = picks[k]
         loads[k, m] = pltpu.make_async_copy(
             (gm, um, dm)[m].at[e, pl.ds(pl.multiple_of(half * H, H), H), :],
-            mv.at[m, k], ld_sem.at[5 if k > 3 else 4 if m == 2 else k],
+            mvd.at[k - 6] if k > 5 else mv.at[m, k],
+            ld_sem.at[6 if k > 5 else 5 if k > 3 else 4 if m == 2 else k],
         )
         loads[k, m].start()
 
@@ -244,11 +247,16 @@
         )
 
     def dn_copy(kind, p):
-        at, n = (mate_spans if kind == 2 else far_spans)[p]
+        at, n = far_spans[p]
         there = wd.at[span(f, g, at, n), :]
-        src = there if kind == 0 else sd.at[at : at + n, :]
-        recv = mate_recv.at[p] if kind == 2 else far_recv.at[kind, p]
-        return remote(src, there, to_dn, recv, {"fs": (twin, mate_twin, mate)[kind]})
+        src = there if kind == 0 else sd.at[0, at : at + n, :]
+        return remote(
+            src, there, to_dn, far_recv.at[kind, p], {"fs": (twin, mate_twin)[kind]}
+        )
+
+    def mate_copy(i):
+        half = (g, 1 - g)[i]
+        return remote(sd.at[i], wd.at[span(f, half, 0, H), :], to_dny, mate_recv.at[i], to_mate)
 
     def send_gu(slot, kinds):
         for p in range(GU_CUT):
@@ -261,8 +269,8 @@
                 dn_copy(kind, p).start()
 
     def send_mate():
-        for p in range(len(mate_spans)):
-            dn_copy(2, p).start()
+        for i in range(2):
+            mate_copy(i).start()
 
     def loaded(block, i):
         pltpu.make_async_copy(block, block, ld_sem.at[i]).wait()
@@ -309,9 +317,11 @@
         send_gu(1, (0, 1))
 
     loaded(mv.at[2, :4], 4)
+    loaded(mvd, 6)
     for slot in range(2):
         lanes = slice(slot * Fl, (slot + 1) * Fl)
-        sd[:, lanes] = mv[2, slot].astype(bf16)
+        sd[0, :, lanes] = mv[2, slot].astype(bf16)
+        sd[1, :, lanes] = mvd[slot].astype(bf16)
         wd[cut(f, g, 0, H), lanes] = mv[2, 2 + slot].astype(bf16)
     send_mate()
 
@@ -339,23 +349,16 @@
     def origin(kind):
         return mate if isinstance(kind, int) else far_a if kind is kind_a else far_b
 
-    def mate_forward():
-        for p, (at, n) in enumerate(mate_spans):
-            here = wd.at[span(mate, g, at, n), :]
-            remote(here, here, to_dny, mate_recv.at[p], peer).wait_recv()
-            remote(here, here, to_dny, mate_y.at[p], peer).start()
-
-    def mate_peer():
-        for p, (at, n) in enumerate(mate_spans):
-            there = wd.at[span(mate, 1 - g, at, n), :]
-            remote(there, there, to_dny, mate_y.at[p], peer).wait_recv()
-
-    def far_forward(*pieces):
+    def mate_arrived():
+        for i, half in enumerate((g, 1 - g)):
+            here = wd.at[span(mate, half, 0, H), :]
+            remote(here, here, to_dny, mate_recv.at[i], to_mate).wait_recv()
+
+    def far_forward(kind, *pieces):
         for p in pieces:
-            for kind, s in ((kind_a, far_a), (kind_b, far_b)):
-                here = wd.at[span(s, g, *far_spans[p]), :]
-                remote(here, here, to_dny, far_recv.at[kind, p], peer).wait_recv()
-                remote(here, here, to_dny, far_y.at[kind, p], peer).start()
+            here = wd.at[span(origin(kind), g, *far_spans[p]), :]
+            remote(here, here, to_dny, far_recv.at[kind, p], peer).wait_recv()
+            remote(here, here, to_dny, far_y.at[kind, p], peer).start()
 
     def far_peer(*pieces):
         for p in pieces:
@@ -451,12 +454,13 @@
 
     class Unit:
         def __init__(self, n, u, count, i, x_first):
-            self.n, self.u, self.count, self.i, self.x_first = n, u, count, i, x_first
+            self.n, self.u, self.count, self.x_first = n, u, count, x_first
             self.theirs, self.mine = ((near_theirs, near_mine), (far_theirs, far_mine))[n]
             self.kept = home if n == 0 else jnp.logical_not(home)
             self.at = [u + c for c in range(count)]
-            self.cross = cross(n, u, count, 2 * T if x_first else T, i)
-            self.back = back(n, u, count, i)
+            rows = 2 * T if x_first else T
+            self.cross = [cross(n, at, 1, rows, i + c) for c, at in enumerate(self.at)]
+            self.back = [back(n, at, 1, i + c) for c, at in enumerate(self.at)]
             self.swap = swap(n, u, count, i)
 
         def give(self):
@@ -472,64 +476,57 @@
                 keep[self.n, at] = y[:, c * Fl : (c + 1) * Fl] + sr[self.n, at].astype(f32)
 
         def send(self):
-            if self.x_first:
-                @pl.when(jnp.logical_not(self.kept))
-                def _():
-                    for at in self.at:
+            for at, over_x, over_z in zip(self.at, self.cross, self.back):
+                if self.x_first:
+                    @pl.when(jnp.logical_not(self.kept))
+                    def _():
                         xs[self.n, at] = keep[self.n, at].astype(bf16)
-                    self.cross.start()
-            else:
-                for at in self.at:
+                        over_x.start()
+                else:
                     zs[self.n, at] = keep[self.n, at, mate_rows, :].astype(bf16)
-                self.back.start()
-
-        def second(self):
-            n = self.n
+                    over_z.start()
+
+        def second(self, c=0):
+            n, at, over_x, over_z = self.n, self.at[c], self.cross[c], self.back[c]
             if self.x_first:
                 @pl.when(self.kept)
                 def _():
-                    self.cross.wait_recv()
-                    for at in self.at:
-                        zs[n, at] = (
-                            keep[n, at, mate_rows, :] + xr[n, at, mate_rows, :].astype(f32)
-                        ).astype(bf16)
-                    self.back.start()
+                    over_x.wait_recv()
+                    zs[n, at] = (
+                        keep[n, at, mate_rows, :] + xr[n, at, mate_rows, :].astype(f32)
+                    ).astype(bf16)
+                    over_z.start()
             else:
                 @pl.when(jnp.logical_not(self.kept))
                 def _():
-                    self.back.wait_recv()
-                    for at in self.at:
-                        xs[n, at, :T] = (keep[n, at, mine_rows, :] + zr[n, at].astype(f32)).astype(bf16)
-                    self.cross.start()
+                    over_z.wait_recv()
+                    xs[n, at, :T] = (keep[n, at, mine_rows, :] + zr[n, at].astype(f32)).astype(bf16)
+                    over_x.start()
 
         def last(self):
             n = self.n
 
             @pl.when(self.kept)
             def _():
-                self.back.wait_recv()
-                if not self.x_first:
-                    self.cross.wait_recv()
-                for at in self.at:
+                for at, over_x, over_z in zip(self.at, self.cross, self.back):
+                    over_z.wait_recv()
+                    if not self.x_first:
+                        over_x.wait_recv()
                     other = xr[n, at, mine_rows, :] if self.x_first else xr[n, at, :T]
                     lanes = pl.ds(pl.multiple_of(at * Fl, Fl), Fl)
                     moe[:, lanes] = (
                         keep[n, at, mine_rows, :] + other.astype(f32) + zr[n, at].astype(f32)
                     ).astype(bf16)
 
-    near = [Unit(0, half * per_half, per_half, half, half == 0) for half in range(2)]
+    near = [Unit(0, half * per_half, per_half, half * per_half, NEAR_X[half]) for half in range(2)]
     far = [
-        Unit(1, half * per_half + j, 1, 2 + k * per_half + j, j % 2 == 0)
+        Unit(1, half * per_half + j, 1, units + k * per_half + j, FAR_X[k * per_half + j])
         for k, half in enumerate((g, 1 - g)) for j in range(per_half)
     ]
     pieces = range(len(far_spans))
     first_pieces = [p for p in pieces if far_spans[p][0] < H // 2]
     last_pieces = [p for p in pieces if p not in first_pieces]
 
-    mate_forward()
-    hidden(0)
-    hidden(1)
-
     def near_give(mine_first):
         @pl.when(own_mine if mine_first else jnp.logical_not(own_mine))
         def _():
@@ -541,31 +538,46 @@
         def _():
             for unit in near:
                 unit.sum()
-            near[0].send()
-
+            for unit in near:
+                if unit.x_first:
+                    unit.send()
+
+    hidden(0)
+    hidden(1)
     near_give(False)
+    far_forward(kind_a, 0, 1)
 
     @pl.when(inner)
     def _():
         near_sum(True)
-        mate_peer()
+        mate_arrived()
         near_give(True)
-        far_forward(*first_pieces[:1])
+        far_forward(kind_a, 2, 3, 4)
         near_sum(False)
-        far_forward(*first_pieces[1:])
+        far_forward(kind_b, 0, 1)
 
     @pl.when(jnp.logical_not(inner))
     def _():
-        far_forward(*first_pieces[:1])
+        far_forward(kind_b, 0)
         near_sum(True)
-        far_forward(*first_pieces[1:])
-        mate_peer()
+        far_forward(kind_b, 1)
+        far_forward(kind_a, 2, 3, 4)
+        mate_arrived()
         near_give(True)
+        far_forward(kind_b, 2)
         near_sum(False)
+        far_forward(kind_b, 3)
 
     far[0].give()
-    far_forward(*last_pieces)
-    near[1].send()
+
+    @pl.when(inner)
+    def _():
+        far_forward(kind_b, 2, 3)
+
+    far_forward(kind_b, 4)
+    for unit in near:
+        if not unit.x_first:
+            unit.send()
     far[1].give()
     far[0].sum()
     far[0].send()
@@ -579,7 +591,11 @@
     far[3].give()
     far[3].sum()
     far[3].send()
-    for unit in near + far:
+    near[0].second(0)
+    near[1].second(0)
+    near[1].second(1)
+    near[0].second(1)
+    for unit in far:
         unit.second()
     for unit in far + near:
         unit.last()
@@ -590,11 +606,25 @@
     w_hop.wait_send()
     for block, sem in (
         (wgu.at[:, : 3 * H, :], to_gu), (wgu.at[:, : 3 * H, :], to_guy),
-        (wd.at[: 3 * H, :], to_dn), (wd.at[: 3 * H, :], to_dny),
+        (wd.at[: 2 * H, :], to_dn), (wd.at[: 4 * H, :], to_dny),
         (xt.at[0, :T, :], to_tok), (xt.at[:3], to_tp), (ss, to_swap),
-        (xs.at[0, : 3 * units // 4], to_x), (zs.at[:, : 3 * units // 4], to_z),
     ):
         all_sent(block, sem)
+
+    near_x, far_x = per_half * sum(NEAR_X), sum(FAR_X)
+
+    def blocks(k):
+        return xt.at[0, : k * T * Fl // Dq, :]
+
+    @pl.when(home)
+    def _():
+        all_sent(blocks(units + far_x), to_x)
+        all_sent(blocks(2 * units - far_x), to_z)
+
+    @pl.when(jnp.logical_not(home))
+    def _():
+        all_sent(blocks(units + near_x), to_x)
+        all_sent(blocks(2 * units - near_x), to_z)
 
 
 def finish_kernel(wgu, wd, moe, gate_o, up_o, down_o, moe_o, sems):
@@ -643,8 +673,9 @@
             pltpu.VMEM((1, Dl), f32),
             pltpu.VMEM((Dl, Fl), f32),
             pltpu.VMEM((3, 6, H, Fl), f32),
+            pltpu.VMEM((2, H, Fl), f32),
             pltpu.VMEM((2, H, 2 * Fl), bf16),
-            pltpu.VMEM((H, 2 * Fl), bf16),
+            pltpu.VMEM((2, H, 2 * Fl), bf16),
             pltpu.VMEM((2, 2 * T, 2 * Fl), f32),
             pltpu.VMEM((2 * T, Fl), f32),
             pltpu.VMEM((2, 2 * T, Fl), f32),
@@ -658,12 +689,12 @@
             pltpu.VMEM((2, units, 2 * T, Fl), f32),
             pltpu.VMEM((2, units, T, Fl), bf16),
             pltpu.VMEM((2, units, T, Fl), bf16),
-            dma((4,)), dma((6,)), dma((10,)),
+            dma((4,)), dma((7,)), dma((10,)),
             dma((TOK_CUT,)), dma(()), dma((3, 2, TOK_CUT)),
             dma(gu), dma(gu),
-            dma((len(MATE_CUTS),)), dma((len(MATE_CUTS),)),
+            dma((2,)),
             dma((2, len(FAR_CUTS))), dma((2, len(FAR_CUTS))),
-            dma((2 + units,)), dma((2 + units,)), dma((2 + units,)),
+            dma((2 * units,)), dma((2 * units,)), dma((2 * units,)),
         ],
         compiler_params=pltpu.CompilerParams(
             collective_id=0, has_side_effects=True, vmem_limit_bytes=48 * 1024 * 1024

time: 54 us -> 53.9 us (level)
  no operation moved by 1% of the time
where the time goes in v1:
time: 53.9 us; the launch traced here: 53.7 us
  Pallas kernels  53.1 us (99%)
  between operations  0.64 us (1%)
    pallas_call x1, Pallas kernels, fused(): pl.pallas_call(kernel, out_shape=(pltpu.VMEM((2, D, 2 * Fl), bf16), pltpu...  51.8 us
    pallas_call x1, Pallas kernels, fused(): pl.pallas_call(finish_kernel, out_shape=(serve, serve, serve, jax.ShapeDt...  1.26 us

profile of v1, /device:TPU:0, one launch (start us, length us, event | category | flops | bytes accessed | tf_op | source)
XLA Modules:
  0.0 53.7 jit_solution(11093355178579075324)
XLA Ops:
  0.6 51.8 %shard_map.102 = (bf16[2,2048,256]{2,1,0:T(8,128)(2,1)S(1)}, bf16[2048,256]{1,0:T(8,128)(2,1)S(1)}, bf16[224,512]{1,0:T(8,128)(2,1)S(1)}) custom-call(bf16[224,512]{1,0:T(8,128)(2,1)} %tokens.1, s32[2,224]{1,0:T(2,128)} %bitcast.3, f32[2,224]{1,0:T(2,128)} %bitcast.4, f32[1,512]{1,0:T(1,128)} %bitcast.5, f32[4,512,128]{2,1,0:T(8,128)} %gm.1, ...), custom_call_target="tpu_custom_call" | custom-call | tf_op jit(solution)/shard_map/pallas_call | solution.py:662
  52.5 1.3 %shard_map.103 = (bf16[1,2048,128]{2,1,0:T(8,128)(2,1)}, bf16[1,2048,128]{2,1,0:T(8,128)(2,1)}, bf16[1,2048,128]{2,1,0:T(8,128)(2,1)}, bf16[224,512]{1,0:T(8,128)(2,1)}) custom-call(bf16[2,2048,256]{2,1,0:T(8,128)(2,1)S(1)} %get-tuple-element.7.wgu, bf16[2048,256]{1,0:T(8,128)(2,1)S(1)} %get-tuple-element.8.wd, bf16[224,512]{1,0:T(8,128)(2,1)S(1)} %get-tuple-element.9.moe), custom_call_target="tpu_custom_call" | custom-call | tf_op jit(solution)/shard_map/pallas_call | solution.py:704
